TPU v7x, 512 devices: a whole 4x4x16 slice. The times are simulated.
512 devices in a mesh: kv: 16 (over y, x), tp: 32 (over z, core).
Axes of the slice: x: 4, y: 4, z: 16, core: 2. Of those that a mesh axis runs over, the one named last changes fastest.
Arguments:
- tokens: bfloat16 [3, 4096], P(None, ('kv', 'tp')), may hold values from -40 to 40
- lengths: int32 [3], replicated, may hold values from 1 to 131072, as said below
- attn_gain: float32 [4096], P(('kv', 'tp')), may hold values from 0.1 to 1.9
- w_query: bfloat16 [4096, 2048], P('kv', 'tp'), may hold values from -0.09375 to 0.09375
- w_key: bfloat16 [4096, 128], P('kv'), may hold values from -0.09375 to 0.09375
- w_value: bfloat16 [4096, 128], P('kv'), may hold values from -0.09375 to 0.09375
- w_forget: bfloat16 [4096, 32], replicated, may hold values from -0.09375 to 0.09375
- forget_bias: float32 [32], replicated, may hold values from -4 to 0
- cache_keys: bfloat16 [3, 128, 131072], P(None, None, ('kv', 'tp')), may hold values from -320 to 320
- cache_values: bfloat16 [3, 128, 131072], P(None, None, ('kv', 'tp')), may hold values from -6 to 6
- cache_decay: float32 [3, 32, 131072], P(None, None, ('kv', 'tp')), may hold values from -16388 to 0, as said below
- out_gain: float32 [2048], replicated, may hold values from 0.1 to 1.9
- w_out: bfloat16 [2048, 4096], P('tp', 'kv'), may hold values from -0.125 to 0.125
- mlp_gain: float32 [4096], P(('kv', 'tp')), may hold values from 0.1 to 1.9
- w_gate: bfloat16 [4096, 11264], P('kv', 'tp'), may hold values from -0.09375 to 0.09375
- w_up: bfloat16 [4096, 11264], P('kv', 'tp'), may hold values from -0.09375 to 0.09375
- w_down: bfloat16 [11264, 4096], P('tp', 'kv'), may hold values from -0.0546875 to 0.0546875
Outputs:
- layer_out: bfloat16 [3, 4096], P(None, ('kv', 'tp'))
Inputs may be any that keep to these rules, and one draw needn't show every extreme that they name: Sequence b has lengths[b] live cache positions, 0 to lengths[b] - 1; some sequence has exactly 131072 in every draw. On live positions, cache_decay[b, h, j] is the sum of the log forget gates of sequence b and head h over positions j + 1 to lengths[b] - 1, so it is zero at the last live position and never rises toward earlier positions; it is zero beyond lengths[b].
All inputs are finite; a program needn't handle non-finite values.
Results may differ from a plain program's by a relative error of at most 0.013.
Values may be sent and summed in bfloat16 or wider, within the bound.
A program may use at most 64 MiB of HBM per device.

v0:
```python
import jax
import jax.numpy as jnp
from jax import lax
from jax.sharding import Mesh
from jax.sharding import PartitionSpec as P

QUERY_HEAD_COUNT = 32
HD = 64
KV_HEADS = 2
TP = ("tp_0", "tp_1")
KV = ("kv_0", "kv_1")
KV_TP = ("kv_0", "kv_1", "tp_0", "tp_1")
epsilon = 1e-06
masked_score = -1e30


def sent_to_all(x, axis):
    copies = jnp.broadcast_to(x, (lax.axis_size(axis), *x.shape))
    return lax.all_to_all(copies, axis, split_axis=0, concat_axis=0, tiled=True)


def joined_along(blocks, dim):
    lengths = list(blocks.shape[1:])
    lengths[dim] *= blocks.shape[0]
    return jnp.moveaxis(blocks, 0, dim).reshape(lengths)


def collect(x, axis, dim):
    blocks = sent_to_all(x, axis)
    return joined_along(blocks, dim)


def by_axis(x, axes):
    for axis in axes:
        x = lax.psum(x, axis)
    return x


def all_in_one(x, axis):
    leaves = jax.tree.leaves(x)
    turns = sorted(range(len(leaves)), key=lambda k: -leaves[k].size)
    width = (1, *leaves[turns[0]].shape)[-1]
    lines = [
        jnp.pad(leaves[k].reshape(-1), (0, -leaves[k].size % width)).reshape(-1, width)
        for k in turns
    ]
    both, at, found = (lax.all_gather(jnp.concatenate(lines), axis), 0, {})
    for k, line in zip(turns, lines):
        piece = both[:, at : at + len(line)].reshape(len(both), -1)
        found[k] = piece[:, : leaves[k].size].reshape(-1, *leaves[k].shape)
        at += len(line)
    numbers = iter(range(len(leaves)))
    return jax.tree.map(lambda _: found[next(numbers)], x)


def merged_by_axis(x, axes, combine):
    for axis in axes:
        pieces = all_in_one(x, axis)
        x = jax.tree.map(lambda part: part[0], pieces)
        for k in range(1, lax.axis_size(axis)):
            x = combine(x, jax.tree.map(lambda part: part[k], pieces))
    return x


def in_blocks(x, dim, length):
    lengths = x.shape
    blocks = x.reshape(*lengths[:dim], length, lengths[dim] // length, *lengths[dim + 1 :])
    return jnp.moveaxis(blocks, dim, 0)


def summed_on_arrival(x, axis, dim):
    length = lax.axis_size(axis)
    blocks = lax.all_to_all(in_blocks(x, dim, length), axis, 0, 0, tiled=True)
    return jnp.sum(blocks, axis=0)


def spread_rows(share, gain):
    scaled = (share.astype(jnp.float32) * gain).astype(jnp.bfloat16)
    squares = jnp.sum(jnp.square(share.astype(jnp.float32)), axis=1)
    row_block, square_parts = (
        collect(scaled.astype(jnp.float32), TP, 1).astype(scaled.dtype),
        collect(squares[:, None], TP, 1),
    )
    square_total = jnp.sum(square_parts, axis=1)
    return (row_block, square_total)


def combine_partials(earlier, later):
    top_a, total_a, sums_a = earlier
    top_b, total_b, sums_b = later
    score_top = jnp.maximum(top_a, top_b)
    scale_a = jnp.exp(top_a - score_top)
    scale_b = jnp.exp(top_b - score_top)
    return (
        score_top,
        total_a * scale_a + total_b * scale_b,
        sums_a * scale_a[..., None] + sums_b * scale_b[..., None],
    )


def body(
    tokens,
    lengths,
    attn_gain,
    w_query,
    w_key,
    w_value,
    w_forget,
    forget_bias,
    cache_keys,
    cache_values,
    cache_decay,
    out_gain,
    w_out,
    mlp_gain,
    w_gate,
    w_up,
    w_down,
):
    full_width = tokens.shape[1] * lax.axis_size(KV) * lax.axis_size(TP)
    kv_index = lax.axis_index(KV)
    tp_index = lax.axis_index(TP)
    row_block, square_total = spread_rows(tokens, attn_gain)
    block_rows = row_block.shape[1]
    forget_rows = lax.dynamic_slice_in_dim(w_forget, kv_index * block_rows, block_rows, 0)
    query_part = jnp.dot(row_block, w_query, preferred_element_type=jnp.float32)
    key_part = jnp.dot(row_block, w_key, preferred_element_type=jnp.float32)
    value_part = jnp.dot(row_block, w_value, preferred_element_type=jnp.float32)
    forget_part = jnp.dot(row_block, forget_rows, preferred_element_type=jnp.float32)
    query_sum, key_sum, value_sum, forget_sum, square_total = (
        by_axis(query_part, KV),
        by_axis(key_part, KV),
        by_axis(value_part, KV),
        by_axis(forget_part, KV),
        by_axis(square_total, KV),
    )
    first_rms = lax.rsqrt(square_total / full_width + epsilon)[:, None]
    query_local = (query_sum * first_rms).astype(jnp.bfloat16)
    key_new = (key_sum * first_rms).astype(jnp.bfloat16)
    value_new = (value_sum * first_rms).astype(jnp.bfloat16)
    log_gate = jax.nn.log_sigmoid(forget_sum * first_rms + forget_bias)
    query_all = collect(query_local, TP, 1)
    batch_rows, key_dims, span = cache_keys.shape
    groups = QUERY_HEAD_COUNT // KV_HEADS
    score_scale = HD ** (-0.5)
    query_grouped = query_all.reshape(batch_rows, KV_HEADS, groups, HD)
    keys_grouped = cache_keys.reshape(batch_rows, KV_HEADS, HD, span)
    values_grouped = cache_values.reshape(batch_rows, KV_HEADS, HD, span)
    scores = jnp.einsum(
        "bkgd,bkdj->bkgj", query_grouped, keys_grouped, preferred_element_type=jnp.float32
    ).reshape(batch_rows, QUERY_HEAD_COUNT, span)
    scores = scores * score_scale + cache_decay + log_gate[:, :, None]
    first_slot = (kv_index * lax.axis_size(TP) + tp_index) * span
    token_positions = first_slot + lax.iota(jnp.int32, span)
    is_live = (token_positions[None, :] < lengths[:, None])[:, None, :]
    scores = jnp.where(is_live, scores, masked_score)
    own_score = (
        jnp.einsum(
            "inpo,ino->inp",
            query_grouped,
            key_new.reshape(batch_rows, KV_HEADS, HD),
            preferred_element_type=jnp.float32,
        ).reshape(batch_rows, QUERY_HEAD_COUNT)
        * score_scale
    )
    local_top = jnp.maximum(jnp.max(scores, axis=2), own_score)
    head_count = w_out.shape[0] // HD
    head_start = tp_index * head_count
    weights = jnp.where(is_live, jnp.exp(scores - local_top[:, :, None]), 0.0)
    weight_total = jnp.sum(weights, axis=2)
    rounded = weights.astype(jnp.bfloat16).reshape(batch_rows, KV_HEADS, groups, span)
    value_sums = jnp.einsum(
        "bkgj,bkdj->bkgd", rounded, values_grouped, preferred_element_type=jnp.float32
    ).reshape(batch_rows, QUERY_HEAD_COUNT, HD)
    weight_total, value_sums = (weight_total, value_sums)
    score_top, weight_total, value_sums = merged_by_axis(
        (local_top, weight_total, value_sums), KV_TP, combine_partials
    )
    weight_total = lax.dynamic_slice_in_dim(weight_total, head_start, head_count, 1)
    value_sums = lax.dynamic_slice_in_dim(value_sums, head_start, head_count, 1)
    score_top = lax.dynamic_slice_in_dim(score_top, head_start, head_count, 1)
    own_here = lax.dynamic_slice_in_dim(own_score, head_start, head_count, 1)
    new_values = jnp.repeat(value_new.reshape(batch_rows, KV_HEADS, HD), groups, axis=1)
    new_values = lax.dynamic_slice_in_dim(new_values, head_start, head_count, 1).astype(jnp.float32)
    own_weight = jnp.exp(own_here - score_top)
    heads_out = (value_sums + own_weight[:, :, None] * new_values) / (weight_total + own_weight)[
        :, :, None
    ]
    head_gains = lax.dynamic_slice_in_dim(out_gain, head_start * HD, head_count * HD, 0).reshape(
        head_count, HD
    )
    normed = (
        heads_out
        * lax.rsqrt(jnp.mean(jnp.square(heads_out), axis=2, keepdims=True) + epsilon)
        * head_gains
    )
    normed = normed.astype(jnp.bfloat16).reshape(batch_rows, head_count * HD)
    attn_part = jnp.dot(normed, w_out, preferred_element_type=jnp.float32)
    attn_share = summed_on_arrival(attn_part, TP, 1)
    residual = (tokens.astype(jnp.float32) + attn_share).astype(jnp.bfloat16)
    mlp_block, mlp_squares = spread_rows(residual, mlp_gain)
    gate_part = jnp.dot(mlp_block, w_gate, preferred_element_type=jnp.float32)
    up_part = jnp.dot(mlp_block, w_up, preferred_element_type=jnp.float32)
    gate_sum, up_sum, mlp_squares = (
        by_axis(gate_part, KV),
        by_axis(up_part, KV),
        by_axis(mlp_squares, KV),
    )
    second_rms = lax.rsqrt(mlp_squares / full_width + epsilon)[:, None]
    hidden = (jax.nn.silu(gate_sum * second_rms) * (up_sum * second_rms)).astype(jnp.bfloat16)
    down_part = jnp.dot(hidden, w_down, preferred_element_type=jnp.float32)
    mlp_share = summed_on_arrival(down_part, TP, 1)
    return (residual.astype(jnp.float32) + mlp_share).astype(jnp.bfloat16)


def solution(mesh):
    torus = Mesh(mesh.devices.reshape(4, 4, 16, 2), ("kv_0", "kv_1", "tp_0", "tp_1"))
    placed = (
        P(None, KV_TP),
        P(),
        P(KV_TP),
        P(KV, TP),
        P(KV, None),
        P(KV, None),
        P(),
        P(),
        P(None, None, KV_TP),
        P(None, None, KV_TP),
        P(None, None, KV_TP),
        P(),
        P(TP, KV),
        P(KV_TP),
        P(KV, TP),
        P(KV, TP),
        P(TP, KV),
    )
    return jax.shard_map(
        body, mesh=torus, in_specs=placed, out_specs=P(None, KV_TP), check_vma=False
    )
```

profile of v0, /device:TPU:1, one launch (start us, length us, event | category | flops | bytes accessed | tf_op | source)
XLA Modules:
  0.0 252.3 jit_solution(7297757308476043918)
XLA Ops:
  0.0 0.8 copy.80
  0.9 0.6 broadcast_in_dim.32
  1.5 16.7 %all-to-all-start.1 = ((f32[32,3,1]{1,2,0:T(1,128)}), f32[32,3,1]{1,2,0:T(1,128)S(1)}, u32[]{:S(2)}, u32[]{:S(2)}) async-start(f32[32,3,1]{1,2,0:T(1,128)} %broadcast_in_dim.32), calls=%async_computation.1 | async-start | bytes 32768 | tf_op jit(solution)/shard_map/all_to_all | solution.py:19
  18.4 11.6 %all-to-all-done.1 = f32[32,3,1]{1,2,0:T(1,128)S(1)} async-done(((f32[32,3,1]{1,2,0:T(1,128)}), f32[32,3,1]{1,2,0:T(1,128)S(1)}, u32[]{:S(2)}, u32[]{:S(2)}) %all-to-all-start.1) | async-done | bytes 416 | tf_op jit(solution)/shard_map/all_to_all | solution.py:19
  30.0 0.6 broadcast_in_dim.31
  30.6 4.6 %all-to-all-start = ((bf16[32,3,8]{2,1,0:T(4,128)(2,1)}), bf16[32,3,8]{2,1,0:T(4,128)(2,1)S(1)}, u32[]{:S(2)}, u32[]{:S(2)}) async-start(bf16[32,3,8]{2,1,0:T(4,128)(2,1)} %broadcast_in_dim.31), calls=%async_computation | async-start | bytes 65536 | tf_op jit(solution)/shard_map/all_to_all | solution.py:19
  35.3 0.1 copy.103
  35.4 0.8 dynamic_slice.27
  36.2 11.2 %all-to-all-done = bf16[32,3,8]{2,1,0:T(4,128)(2,1)S(1)} async-done(((bf16[32,3,8]{2,1,0:T(4,128)(2,1)}), bf16[32,3,8]{2,1,0:T(4,128)(2,1)S(1)}, u32[]{:S(2)}, u32[]{:S(2)}) %all-to-all-start) | async-done | bytes 1568 | tf_op jit(solution)/shard_map/all_to_all | solution.py:19
  47.5 0.1 convert_element_type.81
  47.6 0.1 fusion.200
  47.7 0.1 fusion.201
  47.8 0.5 copy-done.7
  48.3 0.1 fusion.204
  48.4 0.1 fusion.67
  48.6 8.9 %all-reduce.11 = (f32[3,128]{1,0:T(4,128)S(1)}, f32[3]{0:T(128)S(1)}, f32[3,64]{1,0:T(4,128)S(1)}, f32[3,32]{1,0:T(4,128)S(1)}, f32[3,128]{1,0:T(4,128)S(1)}) all-reduce(f32[3,128]{1,0:T(4,128)S(1)} %fusion.204, f32[3]{0:T(128)S(1)} %reduce_sum.73, ...), channel_id=1, replica_groups=mesh['kv_0'=4,'kv_1'=4,'tp_0'=16,'tp_1'=2] {'kv_0'}, use_global_device_ids=true, to_apply=%region_12.13 | all-reduce | flops 1059 | bytes 8472 | tf_op jit(solution)/shard_map/psum | solution.py:35
  57.5 8.7 %all-reduce.9 = (f32[3,128]{1,0:T(4,128)S(1)}, f32[3]{0:T(128)S(1)}, f32[3,64]{1,0:T(4,128)S(1)}, f32[3,32]{1,0:T(4,128)S(1)}, f32[3,128]{1,0:T(4,128)S(1)}) all-reduce(f32[3,128]{1,0:T(4,128)S(1)} %get-tuple-element.22, f32[3]{0:T(128)S(1)} %get-tuple-element.23, ...), channel_id=1, replica_groups=mesh['kv_0'=4,'kv_1'=4,'tp_0'=16,'tp_1'=2] {'kv_1'}, use_global_device_ids=true, to_apply=%region_13.14 | all-reduce | flops 1059 | bytes 8472 | tf_op jit(solution)/shard_map/psum | solution.py:35
  66.3 0.6 broadcast_in_dim.33
  66.9 8.6 %all-to-all-start.2 = ((bf16[32,3,64]{2,1,0:T(4,128)(2,1)}), bf16[32,3,64]{2,1,0:T(4,128)(2,1)S(1)}, u32[]{:S(2)}, u32[]{:S(2)}) async-start(bf16[32,3,64]{2,1,0:T(4,128)(2,1)} %broadcast_in_dim.33), calls=%async_computation.2 | async-start | bytes 65536 | tf_op jit(solution)/shard_map/all_to_all | solution.py:19
  75.5 0.7 copy-done.12
  76.4 11.3 %all-to-all-done.2 = bf16[32,3,64]{2,1,0:T(4,128)(2,1)S(1)} async-done(((bf16[32,3,64]{2,1,0:T(4,128)(2,1)}), bf16[32,3,64]{2,1,0:T(4,128)(2,1)S(1)}, u32[]{:S(2)}, u32[]{:S(2)}) %all-to-all-start.2) | async-done | bytes 12320 | tf_op jit(solution)/shard_map/all_to_all | solution.py:19
  87.7 0.1 fusion.202
  88.0 0.1 convolution_multiply_fusion
  88.2 0.8 copy-done.5
  89.2 0.2 fusion.2
  89.4 0.6 copy-done.2
  89.9 0.1 fusion.203
  90.3 0.1 copy.85
  90.6 0.1 copy.86
  90.8 9.1 %all-gather.4 = f32[4,100,64]{1,2,0:T(8,128)S(1)} all-gather(f32[1,100,64]{1,2,0:T(8,128)S(1)} %maximum_bitcast_fusion), channel_id=2, replica_groups=mesh['kv_0'=4,'kv_1'=4,'tp_0'=16,'tp_1'=2] {'kv_0'}, dimensions={0}, use_global_device_ids=true | all-gather | bytes 128000 | tf_op jit(solution)/shard_map/all_gather | solution.py:47
  99.9 0.1 fusion.197
  100.2 0.1 copy.88
  100.5 0.1 copy.89
  100.7 0.1 copy.90
  100.9 9.1 %all-gather.5 = f32[4,100,64]{1,2,0:T(8,128)S(1)} all-gather(f32[1,100,64]{1,2,0:T(8,128)S(1)} %maximum_bitcast_fusion.1), channel_id=3, replica_groups=mesh['kv_0'=4,'kv_1'=4,'tp_0'=16,'tp_1'=2] {'kv_1'}, dimensions={0}, use_global_device_ids=true | all-gather | bytes 128000 | tf_op jit(solution)/shard_map/all_gather | solution.py:47
  110.0 0.1 fusion.196
  110.3 0.1 copy.92
  110.8 0.1 copy.94
  111.0 22.9 %all-gather.6 = f32[16,100,64]{1,2,0:T(8,128)S(1)} all-gather(f32[1,100,64]{1,2,0:T(8,128)S(1)} %maximum_bitcast_fusion.2), channel_id=4, replica_groups=mesh['kv_0'=4,'kv_1'=4,'tp_0'=16,'tp_1'=2] {'tp_0'}, dimensions={0}, use_global_device_ids=true | all-gather | bytes 435200 | tf_op jit(solution)/shard_map/all_gather | solution.py:47
  133.9 0.3 fusion.195
  134.2 0.2 copy.95
  134.6 0.2 copy.96
  135.2 0.1 copy.98
  135.5 15.0 %all-gather.7 = f32[2,100,64]{1,2,0:T(8,128)S(1)} all-gather(f32[1,100,64]{1,2,0:T(8,128)S(1)} %maximum_bitcast_fusion.3), channel_id=5, replica_groups=mesh['kv_0'=4,'kv_1'=4,'tp_0'=16,'tp_1'=2] {'tp_1'}, dimensions={0}, use_global_device_ids=true | all-gather | bytes 76800 | tf_op jit(solution)/shard_map/all_gather | solution.py:47
  151.7 0.2 fusion.177
  151.9 0.2 multiply_reduce_fusion
  152.2 0.2 convolution_bitcast_fusion
  152.3 0.1 copy.105
  152.5 17.7 %all_to_all.35 = f32[32,3,8]{2,1,0:T(4,128)S(1)} all-to-all(f32[32,3,8]{2,1,0:T(4,128)S(1)} %copy.105), channel_id=1, replica_groups=mesh['kv_0'=4,'kv_1'=4,'tp_0'=16,'tp_1'=2] {'tp_0','tp_1'}, dimensions={0} | all-to-all | bytes 6144 | tf_op jit(solution)/shard_map/all_to_all | solution.py:73
  170.4 0.6 broadcast_in_dim.38
  171.0 5.1 %all-to-all-start.5 = ((f32[32,3,1]{1,2,0:T(1,128)}), f32[32,3,1]{1,2,0:T(1,128)S(1)}, u32[]{:S(2)}, u32[]{:S(2)}) async-start(f32[32,3,1]{1,2,0:T(1,128)} %broadcast_in_dim.38), calls=%async_computation.5 | async-start | bytes 32768 | tf_op jit(solution)/shard_map/all_to_all | solution.py:19
  176.3 11.7 %all-to-all-done.5 = f32[32,3,1]{1,2,0:T(1,128)S(1)} async-done(((f32[32,3,1]{1,2,0:T(1,128)}), f32[32,3,1]{1,2,0:T(1,128)S(1)}, u32[]{:S(2)}, u32[]{:S(2)}) %all-to-all-start.5) | async-done | bytes 416 | tf_op jit(solution)/shard_map/all_to_all | solution.py:19
  188.0 0.6 broadcast_in_dim.37
  188.6 4.5 %all-to-all-start.4 = ((bf16[32,3,8]{2,1,0:T(4,128)(2,1)}), bf16[32,3,8]{2,1,0:T(4,128)(2,1)S(1)}, u32[]{:S(2)}, u32[]{:S(2)}) async-start(bf16[32,3,8]{2,1,0:T(4,128)(2,1)} %broadcast_in_dim.37), calls=%async_computation.4 | async-start | bytes 65536 | tf_op jit(solution)/shard_map/all_to_all | solution.py:19
  193.2 12.2 %all-to-all-done.4 = bf16[32,3,8]{2,1,0:T(4,128)(2,1)S(1)} async-done(((bf16[32,3,8]{2,1,0:T(4,128)(2,1)}), bf16[32,3,8]{2,1,0:T(4,128)(2,1)S(1)}, u32[]{:S(2)}, u32[]{:S(2)}) %all-to-all-start.4) | async-done | bytes 1568 | tf_op jit(solution)/shard_map/all_to_all | solution.py:19
  205.4 0.1 convert_element_type.94
  205.5 0.1 fusion.205
  205.7 0.2 fusion.206
  205.8 10.8 %all-reduce.10 = (f32[3,352]{1,0:T(4,128)S(1)}, f32[3,352]{1,0:T(4,128)S(1)}, f32[3]{0:T(128)S(1)}) all-reduce(f32[3,352]{1,0:T(4,128)S(1)} %fusion.206, f32[3,352]{1,0:T(4,128)S(1)} %fusion.205, f32[3]{0:T(128)S(1)} %reduce_sum.78), channel_id=1, replica_groups=mesh['kv_0'=4,'kv_1'=4,'tp_0'=16,'tp_1'=2] {'kv_0'}, use_global_device_ids=true, to_apply=%region_22.23 | all-reduce | flops 2115 | bytes 16920 | tf_op jit(solution)/shard_map/psum | solution.py:35
  216.7 11.1 %all-reduce.8 = (f32[3,352]{1,0:T(4,128)S(1)}, f32[3,352]{1,0:T(4,128)S(1)}, f32[3]{0:T(128)S(1)}) all-reduce(f32[3,352]{1,0:T(4,128)S(1)} %get-tuple-element.19, f32[3,352]{1,0:T(4,128)S(1)} %get-tuple-element.20, f32[3]{0:T(128)S(1)} %get-tuple-element.21), channel_id=1, replica_groups=mesh['kv_0'=4,'kv_1'=4,'tp_0'=16,'tp_1'=2] {'kv_1'}, use_global_device_ids=true, to_apply=%region_23.24 | all-reduce | flops 2115 | bytes 16920 | tf_op jit(solution)/shard_map/psum | solution.py:35
  227.8 0.2 fusion.77
  228.0 0.1 reshape.1689
  228.2 23.3 %all_to_all.36 = f32[32,3,8]{2,1,0:T(4,128)S(1)} all-to-all(f32[32,3,8]{2,1,0:T(4,128)S(1)} %copy.109), channel_id=1, replica_groups=mesh['kv_0'=4,'kv_1'=4,'tp_0'=16,'tp_1'=2] {'tp_0','tp_1'}, dimensions={0} | all-to-all | bytes 6144 | tf_op jit(solution)/shard_map/all_to_all | solution.py:73
  251.7 0.7 copy.111
  (117 shorter events, 5.3 us)
Async XLA Ops:
  0.0 48.4 %copy-start = (bf16[4096,32]{0,1:T(8,128)(2,1)S(1)}, bf16[4096,32]{0,1:T(8,128)(2,1)}, u32[]{:S(2)}) copy-start(bf16[4096,32]{0,1:T(8,128)(2,1)} %param.23) | copy-start | bytes 786436
  0.0 0.8 copy-start.10
  1.5 28.5 %all-to-all-start.1 = ((f32[32,3,1]{1,2,0:T(1,128)}), f32[32,3,1]{1,2,0:T(1,128)S(1)}, u32[]{:S(2)}, u32[]{:S(2)}) async-start(f32[32,3,1]{1,2,0:T(1,128)} %broadcast_in_dim.32), calls=%async_computation.1 | async-start | bytes 32768 | tf_op jit(solution)/shard_map/all_to_all | solution.py:19
  30.6 4.6 %copy-start.11 = (s32[3]{0:T(128)S(1)}, s32[3]{0:T(128)}, u32[]{:S(2)}) copy-start(s32[3]{0:T(128)} %param.18) | copy-start | bytes 40
  30.6 4.7 %copy-start.8 = (bf16[64,256]{1,0:T(8,128)(2,1)S(1)}, bf16[64,256]{1,0:T(8,128)(2,1)}, u32[]{:S(2)}) copy-start(bf16[64,256]{1,0:T(8,128)(2,1)} %param.29) | copy-start | bytes 98308
  30.6 16.8 %all-to-all-start = ((bf16[32,3,8]{2,1,0:T(4,128)(2,1)}), bf16[32,3,8]{2,1,0:T(4,128)(2,1)S(1)}, u32[]{:S(2)}, u32[]{:S(2)}) async-start(bf16[32,3,8]{2,1,0:T(4,128)(2,1)} %broadcast_in_dim.31), calls=%async_computation | async-start | bytes 65536 | tf_op jit(solution)/shard_map/all_to_all | solution.py:19
  36.2 11.4 %copy-start.9 = (bf16[256,64]{0,1:T(8,128)(2,1)S(1)}, bf16[256,64]{0,1:T(8,128)(2,1)}, u32[]{:S(2)}) copy-start(bf16[256,64]{0,1:T(8,128)(2,1)} %param.20) | copy-start | bytes 98308
  36.2 11.5 %copy-start.6 = (bf16[256,128]{1,0:T(8,128)(2,1)S(1)}, bf16[256,128]{1,0:T(8,128)(2,1)}, u32[]{:S(2)}) copy-start(bf16[256,128]{1,0:T(8,128)(2,1)} %param.21) | copy-start | bytes 196612
  47.5 0.8 copy-start.7
  48.3 39.7 %copy-start.1 = (bf16[3,128,256]{2,1,0:T(8,128)(2,1)S(1)}, bf16[3,128,256]{2,1,0:T(8,128)(2,1)}, u32[]{:S(2)}) copy-start(bf16[3,128,256]{2,1,0:T(8,128)(2,1)} %param.25) | copy-start | bytes 589828
  66.9 20.8 %all-to-all-start.2 = ((bf16[32,3,64]{2,1,0:T(4,128)(2,1)}), bf16[32,3,64]{2,1,0:T(4,128)(2,1)S(1)}, u32[]{:S(2)}, u32[]{:S(2)}) async-start(bf16[32,3,64]{2,1,0:T(4,128)(2,1)} %broadcast_in_dim.33), calls=%async_computation.2 | async-start | bytes 65536 | tf_op jit(solution)/shard_map/all_to_all | solution.py:19
  75.5 0.7 copy-start.12
  88.0 0.9 copy-start.5
  89.0 0.9 copy-start.2
  152.5 23.6 %copy-start.13 = (f32[8]{0:T(128)S(1)}, f32[8]{0:T(128)}, u32[]{:S(2)}) copy-start(f32[8]{0:T(128)} %param.30) | copy-start | bytes 100
  170.2 35.3 %copy-start.3 = (bf16[256,352]{0,1:T(8,128)(2,1)S(1)}, bf16[256,352]{0,1:T(8,128)(2,1)}, u32[]{:S(2)}) copy-start(bf16[256,352]{0,1:T(8,128)(2,1)} %param.31) | copy-start | bytes 540676
  171.0 17.0 %all-to-all-start.5 = ((f32[32,3,1]{1,2,0:T(1,128)}), f32[32,3,1]{1,2,0:T(1,128)S(1)}, u32[]{:S(2)}, u32[]{:S(2)}) async-start(f32[32,3,1]{1,2,0:T(1,128)} %broadcast_in_dim.38), calls=%async_computation.5 | async-start | bytes 32768 | tf_op jit(solution)/shard_map/all_to_all | solution.py:19
  188.6 17.0 %copy-start.4 = (bf16[256,352]{0,1:T(8,128)(2,1)S(1)}, bf16[256,352]{0,1:T(8,128)(2,1)}, u32[]{:S(2)}) copy-start(bf16[256,352]{0,1:T(8,128)(2,1)} %param.32) | copy-start | bytes 540676
  188.6 16.8 %all-to-all-start.4 = ((bf16[32,3,8]{2,1,0:T(4,128)(2,1)}), bf16[32,3,8]{2,1,0:T(4,128)(2,1)S(1)}, u32[]{:S(2)}, u32[]{:S(2)}) async-start(bf16[32,3,8]{2,1,0:T(4,128)(2,1)} %broadcast_in_dim.37), calls=%async_computation.4 | async-start | bytes 65536 | tf_op jit(solution)/shard_map/all_to_all | solution.py:19
  205.5 22.3 %copy-start.14 = (bf16[352,256]{1,0:T(8,128)(2,1)S(1)}, bf16[352,256]{1,0:T(8,128)(2,1)}, u32[]{:S(2)}) copy-start(bf16[352,256]{1,0:T(8,128)(2,1)} %param.33) | copy-start | bytes 540676
where the time goes:
time: 253 us; the launch traced here: 252 us
  blocking collectives  137 us (54%)
  waiting for transfers between devices  58.1 us (23%)
  starting transfers between devices  39.5 us (16%)
  local copies, waits for them, and re-layouts  13.8 us (5%)
    all_to_all x5, waiting for transfers between devices, sent_to_all(): return lax.all_to_all(copies, axis, split_axis=0, concat_axis=0, tiled=True)  58.1 us
    all_gather x4, blocking collectives, all_in_one(): both, at, found = (lax.all_gather(jnp.concatenate(lines), axis), 0, {})  56.1 us
    all_to_all x2, blocking collectives, summed_on_arrival(): blocks = lax.all_to_all(in_blocks(x, dim, length), axis, 0, 0, tiled=True)  41.1 us
    psum x4, blocking collectives, by_axis(): x = lax.psum(x, axis)  39.6 us
    all_to_all x5, starting transfers between devices, sent_to_all(): return lax.all_to_all(copies, axis, split_axis=0, concat_axis=0, tiled=True)  39.5 us
  transfers between devices with their start and end apart: 5, of which 5 were waited for; matrix products, arithmetic and copies ran while one was open for 1% of the time, Pallas kernels for 0%

commit v1 on v0

--- a/solution.py
+++ b/solution.py
@@ -32,7 +32,7 @@
 
 def by_axis(x, axes):
     for axis in axes:
-        x = lax.psum(x, axis)
+        x = jnp.sum(lax.all_gather(x, axis), axis=0)
     return x
 
 

time: 253 us -> 361 us (1.43)
  blocking collectives: 137 us -> 254 us
  waiting for transfers between devices: 58.1 us -> 24.3 us
  starting transfers between devices: 39.5 us -> 58.4 us
  local copies, waits for them, and re-layouts: 13.8 us -> 17.8 us
    all_gather x0 -> x12, blocking collectives: none -> 102 us  [by_axis(): x = jnp.sum(lax.all_gather(x, axis), axis=0)]
    psum x4 -> x0, blocking collectives: 39.6 us -> none  [by_axis(): x = lax.psum(x, axis)]
    all_to_all x5, waiting for transfers between devices: 58.1 us -> 24.3 us  [sent_to_all(): return lax.all_to_all(copies, axis, split_axis=0, concat_axis=0, tiled=True)]
    unnamed x0 -> x4, blocking collectives: none -> 30.3 us
    all_to_all x5, starting transfers between devices: 39.5 us -> 58.4 us  [sent_to_all(): return lax.all_to_all(copies, axis, split_axis=0, concat_axis=0, tiled=True)]
    all_to_all x2, blocking collectives: 41.1 us -> 54.5 us  [summed_on_arrival(): blocks = lax.all_to_all(in_blocks(x, dim, length), axis, 0, 0, tiled=True)]
    all_gather x4, blocking collectives: 56.1 us -> 67.5 us  [all_in_one(): both, at, found = (lax.all_gather(jnp.concatenate(lines), axis), 0, {})]
    unnamed x35 -> x45, local copies, waits for them, and re-layouts: 3.67 us -> 7.26 us
  transfers between devices with their start and end apart: 5 -> 5, of which waited for: 5 -> 3; matrix products, arithmetic and copies ran while one was open for 1% -> 1% of each run, Pallas kernels for 0% -> 0%
where the time goes in v1:
time: 361 us; the launch traced here: 360 us
  blocking collectives  254 us (70%)
  starting transfers between devices  58.4 us (16%)
  waiting for transfers between devices  24.3 us (7%)
  local copies, waits for them, and re-layouts  17.8 us (5%)
    all_gather x12, blocking collectives, by_axis(): x = jnp.sum(lax.all_gather(x, axis), axis=0)  102 us
    all_gather x4, blocking collectives, all_in_one(): both, at, found = (lax.all_gather(jnp.concatenate(lines), axis), 0, {})  67.5 us
    all_to_all x5, starting transfers between devices, sent_to_all(): return lax.all_to_all(copies, axis, split_axis=0, concat_axis=0, tiled=True)  58.4 us
    all_to_all x2, blocking collectives, summed_on_arrival(): blocks = lax.all_to_all(in_blocks(x, dim, length), axis, 0, 0, tiled=True)  54.5 us
    unnamed x4, blocking collectives  30.3 us
    all_to_all x5, waiting for transfers between devices, sent_to_all(): return lax.all_to_all(copies, axis, split_axis=0, concat_axis=0, tiled=True)  24.3 us
    unnamed x45, local copies, waits for them, and re-layouts  7.26 us
  transfers between devices with their start and end apart: 5, of which 3 were waited for; matrix products, arithmetic and copies ran while one was open for 1% of the time, Pallas kernels for 0%

profile of v1, /device:TPU:1, one launch (start us, length us, event | category | flops | bytes accessed | tf_op | source)
XLA Modules:
  0.0 360.2 jit_solution(9235992510378750839)
XLA Ops:
  0.0 0.8 copy.79
  0.9 0.6 broadcast_in_dim.32
  1.5 16.7 %all-to-all-start.1 = ((f32[32,3,1]{1,2,0:T(1,128)}), f32[32,3,1]{1,2,0:T(1,128)S(1)}, u32[]{:S(2)}, u32[]{:S(2)}) async-start(f32[32,3,1]{1,2,0:T(1,128)} %broadcast_in_dim.32), calls=%async_computation.1 | async-start | bytes 32768 | tf_op jit(solution)/shard_map/all_to_all | solution.py:19
  18.3 0.6 copy-done.11
  19.1 1.3 dynamic-slice
  20.4 1.3 dynamic-slice.1
  23.1 7.0 %all-to-all-done.1 = f32[32,3,1]{1,2,0:T(1,128)S(1)} async-done(((f32[32,3,1]{1,2,0:T(1,128)}), f32[32,3,1]{1,2,0:T(1,128)S(1)}, u32[]{:S(2)}, u32[]{:S(2)}) %all-to-all-start.1) | async-done | bytes 416 | tf_op jit(solution)/shard_map/all_to_all | solution.py:19
  30.0 0.6 broadcast_in_dim.31
  30.6 5.2 %all-to-all-start = ((bf16[32,3,8]{2,1,0:T(4,128)(2,1)}), bf16[32,3,8]{2,1,0:T(4,128)(2,1)S(1)}, u32[]{:S(2)}, u32[]{:S(2)}) async-start(bf16[32,3,8]{2,1,0:T(4,128)(2,1)} %broadcast_in_dim.31), calls=%async_computation | async-start | bytes 65536 | tf_op jit(solution)/shard_map/all_to_all | solution.py:19
  35.9 0.2 dynamic-update-slice
  36.2 9.3 %all-reduce.8 = f32[12]{0:T(128)S(1)} all-reduce(f32[12]{0:T(128)S(1)} %dynamic-update-slice), channel_id=4, replica_groups=mesh['kv_0'=4,'kv_1'=4,'tp_0'=16,'tp_1'=2] {'kv_0'}, use_global_device_ids=true, to_apply=%add.8 | all-reduce | flops 12 | bytes 96
  45.6 0.2 dynamic-update-slice.1
  45.8 0.8 dynamic_slice.27
  46.6 8.4 %all-reduce.9 = f32[12]{0:T(128)S(1)} all-reduce(f32[12]{0:T(128)S(1)} %dynamic-update-slice.1), channel_id=5, replica_groups=mesh['kv_0'=4,'kv_1'=4,'tp_0'=16,'tp_1'=2] {'kv_1'}, use_global_device_ids=true, to_apply=%add.9 | all-reduce | flops 12 | bytes 96
  55.2 0.1 convolution_bitcast_fusion.5
  55.4 8.1 %all-gather.22 = f32[4,3,32]{2,1,0:T(4,128)S(1)} all-gather(f32[1,3,32]{2,1,0:T(4,128)S(1)} %convolution_bitcast_fusion.5), channel_id=6, replica_groups=mesh['kv_0'=4,'kv_1'=4,'tp_0'=16,'tp_1'=2] {'kv_0'}, dimensions={0}, use_global_device_ids=true | all-gather | bytes 1920 | tf_op jit(solution)/shard_map/all_gather | solution.py:35
  63.5 8.1 %all-gather.23 = f32[4,3,32]{2,1,0:T(4,128)S(1)} all-gather(f32[1,3,32]{2,1,0:T(4,128)S(1)} %bitcast.777), channel_id=7, replica_groups=mesh['kv_0'=4,'kv_1'=4,'tp_0'=16,'tp_1'=2] {'kv_1'}, dimensions={0}, use_global_device_ids=true | all-gather | bytes 1920 | tf_op jit(solution)/shard_map/all_gather | solution.py:35
  71.8 8.1 %all-gather.20 = f32[4,3,64]{2,1,0:T(4,128)S(1)} all-gather(f32[1,3,64]{2,1,0:T(4,128)S(1)} %convolution_bitcast_fusion.6), channel_id=2, replica_groups=mesh['kv_0'=4,'kv_1'=4,'tp_0'=16,'tp_1'=2] {'kv_0'}, dimensions={0}, use_global_device_ids=true | all-gather | bytes 3840 | tf_op jit(solution)/shard_map/all_gather | solution.py:35
  80.0 8.3 %all-gather.21 = f32[4,3,64]{2,1,0:T(4,128)S(1)} all-gather(f32[1,3,64]{2,1,0:T(4,128)S(1)} %bitcast.778), channel_id=3, replica_groups=mesh['kv_0'=4,'kv_1'=4,'tp_0'=16,'tp_1'=2] {'kv_1'}, dimensions={0}, use_global_device_ids=true | all-gather | bytes 3840 | tf_op jit(solution)/shard_map/all_gather | solution.py:35
  88.3 0.6 broadcast_in_dim.33
  88.9 25.2 %all-to-all-start.2 = ((bf16[32,3,64]{2,1,0:T(4,128)(2,1)}), bf16[32,3,64]{2,1,0:T(4,128)(2,1)S(1)}, u32[]{:S(2)}, u32[]{:S(2)}) async-start(bf16[32,3,64]{2,1,0:T(4,128)(2,1)} %broadcast_in_dim.33), calls=%async_computation.2 | async-start | bytes 65536 | tf_op jit(solution)/shard_map/all_to_all | solution.py:19
  114.2 0.1 convolution_bitcast_fusion.4
  114.3 8.1 %all-gather.24 = f32[4,3,128]{2,1,0:T(4,128)S(1)} all-gather(f32[1,3,128]{2,1,0:T(4,128)S(1)} %convolution_bitcast_fusion.4), channel_id=8, replica_groups=mesh['kv_0'=4,'kv_1'=4,'tp_0'=16,'tp_1'=2] {'kv_0'}, dimensions={0}, use_global_device_ids=true | all-gather | bytes 7680 | tf_op jit(solution)/shard_map/all_gather | solution.py:35
  122.5 8.1 %all-gather.25 = f32[4,3,128]{2,1,0:T(4,128)S(1)} all-gather(f32[1,3,128]{2,1,0:T(4,128)S(1)} %bitcast.779), channel_id=9, replica_groups=mesh['kv_0'=4,'kv_1'=4,'tp_0'=16,'tp_1'=2] {'kv_1'}, dimensions={0}, use_global_device_ids=true | all-gather | bytes 7680 | tf_op jit(solution)/shard_map/all_gather | solution.py:35
  130.8 8.1 %all-gather.30 = f32[4,3,128]{2,1,0:T(4,128)S(1)} all-gather(f32[1,3,128]{2,1,0:T(4,128)S(1)} %convolution_bitcast_fusion.3), channel_id=14, replica_groups=mesh['kv_0'=4,'kv_1'=4,'tp_0'=16,'tp_1'=2] {'kv_0'}, dimensions={0}, use_global_device_ids=true | all-gather | bytes 7680 | tf_op jit(solution)/shard_map/all_gather | solution.py:35
  139.0 8.1 %all-gather.31 = f32[4,3,128]{2,1,0:T(4,128)S(1)} all-gather(f32[1,3,128]{2,1,0:T(4,128)S(1)} %bitcast.780), channel_id=15, replica_groups=mesh['kv_0'=4,'kv_1'=4,'tp_0'=16,'tp_1'=2] {'kv_1'}, dimensions={0}, use_global_device_ids=true | all-gather | bytes 7680 | tf_op jit(solution)/shard_map/all_gather | solution.py:35
  147.3 0.6 copy-done.12
  148.3 0.1 convolution_multiply_fusion
  148.4 0.8 copy-done.5
  149.5 0.2 fusion.2
  149.7 0.6 copy-done.2
  150.2 0.1 fusion.202
  151.0 9.1 %all-gather.26 = f32[4,100,64]{1,2,0:T(8,128)S(1)} all-gather(f32[1,100,64]{1,2,0:T(8,128)S(1)} %maximum_bitcast_fusion), channel_id=10, replica_groups=mesh['kv_0'=4,'kv_1'=4,'tp_0'=16,'tp_1'=2] {'kv_0'}, dimensions={0}, use_global_device_ids=true | all-gather | bytes 128000 | tf_op jit(solution)/shard_map/all_gather | solution.py:47
  160.1 0.1 fusion.199
  161.2 9.4 %all-gather.27 = f32[4,100,64]{1,2,0:T(8,128)S(1)} all-gather(f32[1,100,64]{1,2,0:T(8,128)S(1)} %maximum_bitcast_fusion.1), channel_id=11, replica_groups=mesh['kv_0'=4,'kv_1'=4,'tp_0'=16,'tp_1'=2] {'kv_1'}, dimensions={0}, use_global_device_ids=true | all-gather | bytes 128000 | tf_op jit(solution)/shard_map/all_gather | solution.py:47
  171.6 25.9 %all-gather.28 = f32[16,100,64]{1,2,0:T(8,128)S(1)} all-gather(f32[1,100,64]{1,2,0:T(8,128)S(1)} %maximum_bitcast_fusion.2), channel_id=12, replica_groups=mesh['kv_0'=4,'kv_1'=4,'tp_0'=16,'tp_1'=2] {'tp_0'}, dimensions={0}, use_global_device_ids=true | all-gather | bytes 435200 | tf_op jit(solution)/shard_map/all_gather | solution.py:47
  197.5 0.3 fusion.197
  197.8 0.2 copy.94
  198.1 0.2 copy.95
  199.0 23.1 %all-gather.29 = f32[2,100,64]{1,2,0:T(8,128)S(1)} all-gather(f32[1,100,64]{1,2,0:T(8,128)S(1)} %maximum_bitcast_fusion.3), channel_id=13, replica_groups=mesh['kv_0'=4,'kv_1'=4,'tp_0'=16,'tp_1'=2] {'tp_1'}, dimensions={0}, use_global_device_ids=true | all-gather | bytes 76800 | tf_op jit(solution)/shard_map/all_gather | solution.py:47
  223.3 0.2 fusion.179
  223.5 0.2 multiply_reduce_fusion
  223.8 0.2 convolution_bitcast_fusion
  224.0 0.1 copy.104
  224.1 22.4 %all_to_all.35 = f32[32,3,8]{2,1,0:T(4,128)S(1)} all-to-all(f32[32,3,8]{2,1,0:T(4,128)S(1)} %copy.104), channel_id=1, replica_groups=mesh['kv_0'=4,'kv_1'=4,'tp_0'=16,'tp_1'=2] {'tp_0','tp_1'}, dimensions={0} | all-to-all | bytes 6144 | tf_op jit(solution)/shard_map/all_to_all | solution.py:73
  246.6 0.6 broadcast_in_dim.38
  247.2 5.1 %all-to-all-start.5 = ((f32[32,3,1]{1,2,0:T(1,128)}), f32[32,3,1]{1,2,0:T(1,128)S(1)}, u32[]{:S(2)}, u32[]{:S(2)}) async-start(f32[32,3,1]{1,2,0:T(1,128)} %broadcast_in_dim.38), calls=%async_computation.5 | async-start | bytes 32768 | tf_op jit(solution)/shard_map/all_to_all | solution.py:19
  252.4 11.8 %all-to-all-done.5 = f32[32,3,1]{1,2,0:T(1,128)S(1)} async-done(((f32[32,3,1]{1,2,0:T(1,128)}), f32[32,3,1]{1,2,0:T(1,128)S(1)}, u32[]{:S(2)}, u32[]{:S(2)}) %all-to-all-start.5) | async-done | bytes 416 | tf_op jit(solution)/shard_map/all_to_all | solution.py:19
  264.3 0.2 dynamic-update-slice.2
  264.7 6.0 %all-reduce.10 = f32[12]{0:T(128)S(1)} all-reduce(f32[12]{0:T(128)S(1)} %dynamic-update-slice.2), channel_id=18, replica_groups=mesh['kv_0'=4,'kv_1'=4,'tp_0'=16,'tp_1'=2] {'kv_0'}, use_global_device_ids=true, to_apply=%add.10 | all-reduce | flops 12 | bytes 96
  270.7 0.2 dynamic-update-slice.3
  271.0 0.6 broadcast_in_dim.37
  271.6 6.1 %all-to-all-start.4 = ((bf16[32,3,8]{2,1,0:T(4,128)(2,1)}), bf16[32,3,8]{2,1,0:T(4,128)(2,1)S(1)}, u32[]{:S(2)}, u32[]{:S(2)}) async-start(bf16[32,3,8]{2,1,0:T(4,128)(2,1)} %broadcast_in_dim.37), calls=%async_computation.4 | async-start | bytes 65536 | tf_op jit(solution)/shard_map/all_to_all | solution.py:19
  277.7 6.6 %all-reduce.11 = f32[12]{0:T(128)S(1)} all-reduce(f32[12]{0:T(128)S(1)} %dynamic-update-slice.3), channel_id=19, replica_groups=mesh['kv_0'=4,'kv_1'=4,'tp_0'=16,'tp_1'=2] {'kv_1'}, use_global_device_ids=true, to_apply=%add.11 | all-reduce | flops 12 | bytes 96
  284.4 5.5 %all-to-all-done.4 = bf16[32,3,8]{2,1,0:T(4,128)(2,1)S(1)} async-done(((bf16[32,3,8]{2,1,0:T(4,128)(2,1)}), bf16[32,3,8]{2,1,0:T(4,128)(2,1)S(1)}, u32[]{:S(2)}, u32[]{:S(2)}) %all-to-all-start.4) | async-done | bytes 1568 | tf_op jit(solution)/shard_map/all_to_all | solution.py:19
  290.1 0.1 convolution_bitcast_fusion.2
  290.2 9.1 %all-gather.32 = f32[4,3,352]{2,1,0:T(4,128)S(1)} all-gather(f32[1,3,352]{2,1,0:T(4,128)S(1)} %convolution_bitcast_fusion.2), channel_id=16, replica_groups=mesh['kv_0'=4,'kv_1'=4,'tp_0'=16,'tp_1'=2] {'kv_0'}, dimensions={0}, use_global_device_ids=true | all-gather | bytes 21120 | tf_op jit(solution)/shard_map/all_gather | solution.py:35
  299.3 9.1 %all-gather.33 = f32[4,3,352]{2,1,0:T(4,128)S(1)} all-gather(f32[1,3,352]{2,1,0:T(4,128)S(1)} %bitcast.775), channel_id=17, replica_groups=mesh['kv_0'=4,'kv_1'=4,'tp_0'=16,'tp_1'=2] {'kv_1'}, dimensions={0}, use_global_device_ids=true | all-gather | bytes 21120 | tf_op jit(solution)/shard_map/all_gather | solution.py:35
  308.4 0.1 convolution_bitcast_fusion.1
  308.6 9.1 %all-gather.34 = f32[4,3,352]{2,1,0:T(4,128)S(1)} all-gather(f32[1,3,352]{2,1,0:T(4,128)S(1)} %convolution_bitcast_fusion.1), channel_id=20, replica_groups=mesh['kv_0'=4,'kv_1'=4,'tp_0'=16,'tp_1'=2] {'kv_0'}, dimensions={0}, use_global_device_ids=true | all-gather | bytes 21120 | tf_op jit(solution)/shard_map/all_gather | solution.py:35
  317.7 9.2 %all-gather.35 = f32[4,3,352]{2,1,0:T(4,128)S(1)} all-gather(f32[1,3,352]{2,1,0:T(4,128)S(1)} %bitcast.776), channel_id=21, replica_groups=mesh['kv_0'=4,'kv_1'=4,'tp_0'=16,'tp_1'=2] {'kv_1'}, dimensions={0}, use_global_device_ids=true | all-gather | bytes 21120 | tf_op jit(solution)/shard_map/all_gather | solution.py:35
  327.0 0.2 fusion.76
  327.3 32.1 %all_to_all.36 = f32[32,3,8]{2,1,0:T(4,128)S(1)} all-to-all(f32[32,3,8]{2,1,0:T(4,128)S(1)} %copy.108), channel_id=1, replica_groups=mesh['kv_0'=4,'kv_1'=4,'tp_0'=16,'tp_1'=2] {'tp_0','tp_1'}, dimensions={0} | all-to-all | bytes 6144 | tf_op jit(solution)/shard_map/all_to_all | solution.py:73
  359.6 0.7 copy.110
  (159 shorter events, 7.7 us)
Async XLA Ops:
  0.0 55.2 %copy-start = (bf16[4096,32]{0,1:T(8,128)(2,1)S(1)}, bf16[4096,32]{0,1:T(8,128)(2,1)}, u32[]{:S(2)}) copy-start(bf16[4096,32]{0,1:T(8,128)(2,1)} %param.23) | copy-start | bytes 786436
  0.0 0.8 copy-start.10
  1.5 28.5 %all-to-all-start.1 = ((f32[32,3,1]{1,2,0:T(1,128)}), f32[32,3,1]{1,2,0:T(1,128)S(1)}, u32[]{:S(2)}, u32[]{:S(2)}) async-start(f32[32,3,1]{1,2,0:T(1,128)} %broadcast_in_dim.32), calls=%async_computation.1 | async-start | bytes 32768 | tf_op jit(solution)/shard_map/all_to_all | solution.py:19
  18.3 0.7 copy-start.11
  18.3 4.7 %copy-start.8 = (bf16[64,256]{1,0:T(8,128)(2,1)S(1)}, bf16[64,256]{1,0:T(8,128)(2,1)}, u32[]{:S(2)}) copy-start(bf16[64,256]{1,0:T(8,128)(2,1)} %param.29) | copy-start | bytes 98308
  30.6 24.5 %all-to-all-start = ((bf16[32,3,8]{2,1,0:T(4,128)(2,1)}), bf16[32,3,8]{2,1,0:T(4,128)(2,1)S(1)}, u32[]{:S(2)}, u32[]{:S(2)}) async-start(bf16[32,3,8]{2,1,0:T(4,128)(2,1)} %broadcast_in_dim.31), calls=%async_computation | async-start | bytes 65536 | tf_op jit(solution)/shard_map/all_to_all | solution.py:19
  55.2 16.4 %copy-start.9 = (bf16[256,64]{0,1:T(8,128)(2,1)S(1)}, bf16[256,64]{0,1:T(8,128)(2,1)}, u32[]{:S(2)}) copy-start(bf16[256,64]{0,1:T(8,128)(2,1)} %param.20) | copy-start | bytes 98308
  79.9 34.2 %copy-start.6 = (bf16[256,128]{1,0:T(8,128)(2,1)S(1)}, bf16[256,128]{1,0:T(8,128)(2,1)}, u32[]{:S(2)}) copy-start(bf16[256,128]{1,0:T(8,128)(2,1)} %param.21) | copy-start | bytes 196612
  88.9 41.8 %copy-start.7 = (bf16[256,128]{1,0:T(8,128)(2,1)S(1)}, bf16[256,128]{1,0:T(8,128)(2,1)}, u32[]{:S(2)}) copy-start(bf16[256,128]{1,0:T(8,128)(2,1)} %param.22) | copy-start | bytes 196612
  88.9 59.0 %all-to-all-start.2 = ((bf16[32,3,64]{2,1,0:T(4,128)(2,1)}), bf16[32,3,64]{2,1,0:T(4,128)(2,1)S(1)}, u32[]{:S(2)}, u32[]{:S(2)}) async-start(bf16[32,3,64]{2,1,0:T(4,128)(2,1)} %broadcast_in_dim.33), calls=%async_computation.2 | async-start | bytes 65536 | tf_op jit(solution)/shard_map/all_to_all | solution.py:19
  114.2 34.1 %copy-start.1 = (bf16[3,128,256]{2,1,0:T(8,128)(2,1)S(1)}, bf16[3,128,256]{2,1,0:T(8,128)(2,1)}, u32[]{:S(2)}) copy-start(bf16[3,128,256]{2,1,0:T(8,128)(2,1)} %param.25) | copy-start | bytes 589828
  147.2 0.7 copy-start.12
  148.3 0.9 copy-start.5
  149.3 0.9 copy-start.2
  224.1 28.2 %copy-start.13 = (f32[8]{0:T(128)S(1)}, f32[8]{0:T(128)}, u32[]{:S(2)}) copy-start(f32[8]{0:T(128)} %param.30) | copy-start | bytes 100
  246.5 43.6 %copy-start.3 = (bf16[256,352]{0,1:T(8,128)(2,1)S(1)}, bf16[256,352]{0,1:T(8,128)(2,1)}, u32[]{:S(2)}) copy-start(bf16[256,352]{0,1:T(8,128)(2,1)} %param.31) | copy-start | bytes 540676
  247.2 17.0 %all-to-all-start.5 = ((f32[32,3,1]{1,2,0:T(1,128)}), f32[32,3,1]{1,2,0:T(1,128)S(1)}, u32[]{:S(2)}, u32[]{:S(2)}) async-start(f32[32,3,1]{1,2,0:T(1,128)} %broadcast_in_dim.38), calls=%async_computation.5 | async-start | bytes 32768 | tf_op jit(solution)/shard_map/all_to_all | solution.py:19
  271.6 18.4 %all-to-all-start.4 = ((bf16[32,3,8]{2,1,0:T(4,128)(2,1)}), bf16[32,3,8]{2,1,0:T(4,128)(2,1)S(1)}, u32[]{:S(2)}, u32[]{:S(2)}) async-start(bf16[32,3,8]{2,1,0:T(4,128)(2,1)} %broadcast_in_dim.37), calls=%async_computation.4 | async-start | bytes 65536 | tf_op jit(solution)/shard_map/all_to_all | solution.py:19
  290.0 18.5 %copy-start.4 = (bf16[256,352]{0,1:T(8,128)(2,1)S(1)}, bf16[256,352]{0,1:T(8,128)(2,1)}, u32[]{:S(2)}) copy-start(bf16[256,352]{0,1:T(8,128)(2,1)} %param.32) | copy-start | bytes 540676
  308.4 18.5 %copy-start.14 = (bf16[352,256]{1,0:T(8,128)(2,1)S(1)}, bf16[352,256]{1,0:T(8,128)(2,1)}, u32[]{:S(2)}) copy-start(bf16[352,256]{1,0:T(8,128)(2,1)} %param.33) | copy-start | bytes 540676
